TPU v7x, 32 devices: a whole 2x2x4 slice. The times are simulated.
32 devices in a mesh: sp: 4 (over y, core), dp: 8 (over z, x).
Axes of the slice: x: 2, y: 2, z: 4, core: 2. Of those that a mesh axis runs over, the one named last changes fastest.
Arguments:
- queries: bfloat16 [8, 1024, 1024], P('dp', 'sp'), may hold values from -250 to 250
- keys: bfloat16 [8, 1024, 1024], P('dp', 'sp'), may hold values from -6 to 6
- values: bfloat16 [8, 1024, 1024], P('dp', 'sp'), may hold values from -6 to 6
- cum_gate: float32 [8, 16, 1024], P('dp', 'sp'), may hold values from -1024 to 0, as said below
- out_weight: bfloat16 [1024, 2112], P(None, 'dp'), may hold values from -1.5 to 1.5
Outputs:
- mixed: bfloat16 [8, 1024, 2112], P('dp', 'sp')
Inputs may be any that keep to these rules, and one draw needn't show every extreme that they name: `cum_gate`: within each head the entries do not rise along positions.
All inputs are finite; a program needn't handle non-finite values.
Results may differ from a plain program's by a relative error of at most 0.0053.
Values may be sent and summed in bfloat16 or wider, within the bound.
A program may use at most 64 MiB of HBM per device.

v0:
```python
import jax
import jax.numpy as jnp
from jax import lax
from jax.sharding import PartitionSpec as P


def attend(query_all, key_all, value_all, gate_all):
    length, width = query_all.shape
    heads = gate_all.shape[0]
    depth = width // heads
    block_rows = min(512, length)
    block_count = length // block_rows
    score_scale = depth ** (-0.5)
    query_blocks = query_all.reshape(block_count, block_rows, heads, depth)
    key_blocks = key_all.reshape(block_count, block_rows, heads, depth)
    value_blocks = value_all.reshape(block_count, block_rows, heads, depth)
    gate_blocks = gate_all.reshape(heads, block_count, block_rows).transpose(1, 0, 2)
    offsets = jnp.arange(block_rows, dtype=jnp.int32)

    def one_block(block_index):
        query_part = lax.dynamic_index_in_dim(query_blocks, block_index, 0, keepdims=False)
        gate_part = lax.dynamic_index_in_dim(gate_blocks, block_index, 0, keepdims=False)
        query_rows = block_index * block_rows + offsets

        def key_step(key_block, carry):
            running_max, running_sum, weighted = carry
            key_part = lax.dynamic_index_in_dim(key_blocks, key_block, 0, keepdims=False)
            value_part = lax.dynamic_index_in_dim(value_blocks, key_block, 0, keepdims=False)
            gate_keys = lax.dynamic_index_in_dim(gate_blocks, key_block, 0, keepdims=False)
            logits = (
                jnp.einsum("qhe,khe->hqk", query_part, key_part, preferred_element_type=jnp.float32)
                * score_scale
            )
            logits = logits + gate_part[:, :, None] - gate_keys[:, None, :]
            key_rows = key_block * block_rows + offsets
            allowed = key_rows[None, :] <= query_rows[:, None]
            logits = jnp.where(allowed[None], logits, -jnp.inf)
            new_max = jnp.maximum(running_max, jnp.max(logits, axis=-1))
            scores = jnp.exp(logits - new_max[..., None])
            factor = jnp.exp(running_max - new_max)
            running_sum = running_sum * factor + jnp.sum(scores, axis=-1)
            weighted = weighted * factor[..., None] + jnp.einsum(
                "hqk,khe->hqe",
                scores.astype(jnp.bfloat16),
                value_part,
                preferred_element_type=jnp.float32,
            )
            return (new_max, running_sum, weighted)

        start_state = (
            jnp.full((heads, block_rows), -jnp.inf, jnp.float32),
            jnp.zeros((heads, block_rows), jnp.float32),
            jnp.zeros((heads, block_rows, depth), jnp.float32),
        )
        final_max, final_sum, weighted = lax.fori_loop(0, block_index + 1, key_step, start_state)
        result = weighted / final_sum[..., None]
        return result.transpose(1, 0, 2).astype(jnp.bfloat16)

    outputs = lax.map(one_block, jnp.arange(block_count, dtype=jnp.int32))
    return outputs.reshape(length, width)


def body(queries, keys, values, cum_gate, out_weight):
    query_heads, key_heads, value_heads = (
        lax.all_to_all(queries, "sp", split_axis=2, concat_axis=1, tiled=True),
        lax.all_to_all(keys, "sp", split_axis=2, concat_axis=1, tiled=True),
        lax.all_to_all(values, "sp", split_axis=2, concat_axis=1, tiled=True),
    )
    local_out = attend(query_heads[0], key_heads[0], value_heads[0], cum_gate[0])
    attended = lax.all_to_all(local_out[None], "sp", split_axis=1, concat_axis=2, tiled=True)[0]
    group_rows = attended.shape[1] // lax.axis_size("sp")
    own_rows = lax.dynamic_slice_in_dim(
        out_weight, lax.axis_index("sp") * group_rows, group_rows, 0
    )
    full_rows = lax.all_gather(own_rows, "dp", axis=1, tiled=True)
    whole_weight = lax.all_gather(full_rows, "sp", axis=0, tiled=True)
    mixed = jnp.dot(attended, whole_weight, preferred_element_type=jnp.float32)
    return mixed.astype(jnp.bfloat16)[None]


def solution(mesh):
    in_specs = (
        P("dp", "sp", None),
        P("dp", "sp", None),
        P("dp", "sp", None),
        P("dp", "sp", None),
        P(None, "dp"),
    )
    out_specs = P("dp", "sp", None)
    return jax.shard_map(body, mesh=mesh, in_specs=in_specs, out_specs=out_specs, check_vma=False)
```

profile of v0, /device:TPU:0, one launch (start us, length us, event | category | flops | bytes accessed | tf_op | source)
XLA Modules:
  0.0 110.8 jit_solution(6020720090809697798)
XLA Ops:
  6.5 1.0 copy-done
  8.3 2.4 %copy.29 = bf16[1,256,1024]{1,0,2:T(2,128)(2,1)S(1)} copy(bf16[1,256,1024]{2,1,0:T(8,128)(2,1)} %param.9) | data formatting | bytes 1048576 | tf_op args[0]
  11.2 3.8 %reduce = bf16[1024,256]{1,0:T(8,128)(2,1)S(1)} reduce(bf16[1024,1,256]{2,1,0:T(2,128)(2,1)S(1)} %bitcast.91, bf16[]{:T(256)} %broadcast.54), dimensions={1}, to_apply=%bitcast.52.reduce_sub_computation | reduce | bytes 1048578
  15.0 0.9 reshape.40
  15.9 4.3 %all-to-all-start = ((bf16[4,2,32768]{2,1,0:T(2,128)(2,1)}), bf16[4,2,32768]{2,1,0:T(2,128)(2,1)S(1)}, u32[]{:S(2)}, u32[]{:S(2)}) async-start(bf16[4,2,32768]{2,1,0:T(2,128)(2,1)} %reshape.40), calls=%async_computation | async-start | bytes 1048576 | tf_op jit(solution)/shard_map/all_to_all | solution.py:65
  21.0 3.8 %reduce.1 = bf16[1024,256]{1,0:T(8,128)(2,1)S(1)} reduce(bf16[1024,1,256]{2,1,0:T(2,128)(2,1)S(1)} %bitcast.93, bf16[]{:T(256)} %broadcast.54), dimensions={1}, to_apply=%bitcast.54.reduce_sub_computation | reduce | bytes 1048578
  24.9 0.9 reshape.42
  25.8 3.2 %all-to-all-done = bf16[4,2,32768]{2,1,0:T(2,128)(2,1)S(1)} async-done(((bf16[4,2,32768]{2,1,0:T(2,128)(2,1)}), bf16[4,2,32768]{2,1,0:T(2,128)(2,1)S(1)}, u32[]{:S(2)}, u32[]{:S(2)}) %all-to-all-start) | async-done | bytes 524320 | tf_op jit(solution)/shard_map/all_to_all | solution.py:65
  29.0 3.5 %all-to-all-start.1 = ((bf16[4,2,32768]{2,1,0:T(2,128)(2,1)}), bf16[4,2,32768]{2,1,0:T(2,128)(2,1)S(1)}, u32[]{:S(2)}, u32[]{:S(2)}) async-start(bf16[4,2,32768]{2,1,0:T(2,128)(2,1)} %reshape.42), calls=%async_computation.1 | async-start | bytes 1048576 | tf_op jit(solution)/shard_map/all_to_all | solution.py:66
  32.5 2.4 %copy.33 = bf16[1,256,1024]{1,0,2:T(2,128)(2,1)S(1)} copy(bf16[1,256,1024]{2,1,0:T(8,128)(2,1)} %param.11) | data formatting | bytes 1048576 | tf_op args[2]
  34.9 3.8 %reduce.2 = bf16[1024,256]{1,0:T(8,128)(2,1)S(1)} reduce(bf16[1024,1,256]{2,1,0:T(2,128)(2,1)S(1)} %bitcast.94, bf16[]{:T(256)} %broadcast.54), dimensions={1}, to_apply=%bitcast.56.reduce_sub_computation | reduce | bytes 1048578
  38.7 0.9 reshape.44
  39.6 1.7 %all-to-all-done.1 = bf16[4,2,32768]{2,1,0:T(2,128)(2,1)S(1)} async-done(((bf16[4,2,32768]{2,1,0:T(2,128)(2,1)}), bf16[4,2,32768]{2,1,0:T(2,128)(2,1)S(1)}, u32[]{:S(2)}, u32[]{:S(2)}) %all-to-all-start.1) | async-done | bytes 524320 | tf_op jit(solution)/shard_map/all_to_all | solution.py:66
  41.3 4.1 %all-to-all-start.2 = ((bf16[4,2,32768]{2,1,0:T(2,128)(2,1)}), bf16[4,2,32768]{2,1,0:T(2,128)(2,1)}, u32[]{:S(2)}, u32[]{:S(2)}) async-start(bf16[4,2,32768]{2,1,0:T(2,128)(2,1)} %reshape.44), calls=%async_computation.2 | async-start | bytes 1048576 | tf_op jit(solution)/shard_map/all_to_all | solution.py:67
  48.6 5.7 %all-to-all-done.2 = bf16[4,2,32768]{2,1,0:T(2,128)(2,1)} async-done(((bf16[4,2,32768]{2,1,0:T(2,128)(2,1)}), bf16[4,2,32768]{2,1,0:T(2,128)(2,1)}, u32[]{:S(2)}, u32[]{:S(2)}) %all-to-all-start.2) | async-done | bytes 524320 | tf_op jit(solution)/shard_map/all_to_all | solution.py:67
  54.3 2.2 %reshape.45 = bf16[1024,1,256]{2,1,0:T(2,128)(2,1)S(1)} reshape(bf16[4,2,32768]{2,1,0:T(2,128)(2,1)} %all-to-all-done.2) | data formatting | bytes 1048576
  57.3 0.9 copy.37
  58.3 21.7 %while.29 = (s32[]{:T(128)}, bf16[2,512,4,64]{1,3,2,0:T(8,128)(2,1)S(1)}, s32[2]{0:T(128)S(1)}, bf16[2,512,4,64]{1,3,2,0:T(8,128)(2,1)S(1)}, f32[2,4,512]{2,1,0:...) while((s32[]{:T(128)}, ...), condition=%wide.region_5.6_spmd.clone.clone, body=%wide.region_0.5_spmd.clone.clone.sunk | while | flops 287052800 | bytes 19649152 | solution.py:59
  62.2 4.6 %while.30 = (s32[]{:T(128)}, f32[4,512]{1,0:T(4,128)S(1)}, f32[4,512]{1,0:T(4,128)S(1)}, f32[4,512,64]{1,2,0:T(8,128)S(1)}, s32[]{:T(128)}, /*index=5*/s32[512]{...) while((s32[]{:T(128)}, f32[4,512]{1,0:T(4,128)S(1)}, ...), condition=%wide.region_4.4_spmd, body=%wide.region_1.3_spmd.sunk | while | flops 286790144 | bytes 17768688 | solution.py:55
  62.5 1.3 %fusion.33 = (f32[4,512]{1,0:T(4,128)S(1)}, f32[4,512,512]{2,1,0:T(8,128)S(1)}) fusion(f32[4,512]{1,0:T(4,128)S(1)} %dynamic-slice_bitcast_fusion.8, f32[4,512]{1,0:T(4,128)S(1)} %get-tuple-element.413, pred[512,512]{0,1:T(8,128)(4,1)S(1)} %broadcast_compare_fusion.2, bf16[512,4,64]{0,2,1:T(8,128)(2,1)S(1)} %get-tuple-element.412, ...), kind=kOutput, calls=%fused_computation.5.clone.1 | convolution fusion | flops 139458560 | bytes 5005316 | tf_op jit(solution)/shard_map/while/body/eval_jaxpr/while/body/qhe,khe->hqk/dot_general | solution.py:31
  63.8 1.4 %fusion.34 = f32[4,512]{1,0:T(4,128)S(1)} fusion(f32[4,512,512]{2,1,0:T(8,128)S(1)} %get-tuple-element.369, f32[4,512]{1,0:T(4,128)S(1)} %max.4, f32[4,512]{1,0:T(4,128)S(1)} %dynamic-slice_bitcast_fusion.8, f32[4,512]{1,0:T(4,128)S(1)} %get-tuple-element.413, pred[512,512]{0,1:T(8,128)(4,1)S(1)} %broadcast_compare_fusion.2), kind=kLoop, calls=%fused_computation.4.clone.1 | loop fusion | flops 6289408 | bytes 4489216 | tf_op jit(solution)/shard_map/while/body/eval_jaxpr/while/body/reduce_sum | solution.py:41
  65.2 1.6 %fusion.35 = f32[4,512,64]{1,2,0:T(8,128)S(1)} fusion(f32[4,512,512]{2,1,0:T(8,128)S(1)} %get-tuple-element.369, f32[4,512]{1,0:T(4,128)S(1)} %max.4, f32[4,512]{1,0:T(4,128)S(1)} %dynamic-slice_bitcast_fusion.8, f32[4,512]{1,0:T(4,128)S(1)} %get-tuple-element.413, pred[512,512]{0,1:T(8,128)(4,1)S(1)} %broadcast_compare_fusion.2, ...), kind=kOutput, calls=%fused_computation.8.clone.1 | convolution fusion | flops 140771328 | bytes 5799940 | tf_op jit(solution)/shard_map/while/body/eval_jaxpr/while/body/hqk,khe->hqe/dot_general | solution.py:42
  70.8 9.1 %while.30 = (s32[]{:T(128)}, f32[4,512]{1,0:T(4,128)S(1)}, f32[4,512]{1,0:T(4,128)S(1)}, f32[4,512,64]{1,2,0:T(8,128)S(1)}, s32[]{:T(128)}, /*index=5*/s32[512]{...) while((s32[]{:T(128)}, f32[4,512]{1,0:T(4,128)S(1)}, ...), condition=%wide.region_4.4_spmd, body=%wide.region_1.3_spmd.sunk | while | flops 286790144 | bytes 17768688 | solution.py:55
  71.1 1.3 %fusion.33 = (f32[4,512]{1,0:T(4,128)S(1)}, f32[4,512,512]{2,1,0:T(8,128)S(1)}) fusion(f32[4,512]{1,0:T(4,128)S(1)} %dynamic-slice_bitcast_fusion.8, f32[4,512]{1,0:T(4,128)S(1)} %get-tuple-element.413, pred[512,512]{0,1:T(8,128)(4,1)S(1)} %broadcast_compare_fusion.2, bf16[512,4,64]{0,2,1:T(8,128)(2,1)S(1)} %get-tuple-element.412, ...), kind=kOutput, calls=%fused_computation.5.clone.1 | convolution fusion | flops 139458560 | bytes 5005316 | tf_op jit(solution)/shard_map/while/body/eval_jaxpr/while/body/qhe,khe->hqk/dot_general | solution.py:31
  72.4 1.4 %fusion.34 = f32[4,512]{1,0:T(4,128)S(1)} fusion(f32[4,512,512]{2,1,0:T(8,128)S(1)} %get-tuple-element.369, f32[4,512]{1,0:T(4,128)S(1)} %max.4, f32[4,512]{1,0:T(4,128)S(1)} %dynamic-slice_bitcast_fusion.8, f32[4,512]{1,0:T(4,128)S(1)} %get-tuple-element.413, pred[512,512]{0,1:T(8,128)(4,1)S(1)} %broadcast_compare_fusion.2), kind=kLoop, calls=%fused_computation.4.clone.1 | loop fusion | flops 6289408 | bytes 4489216 | tf_op jit(solution)/shard_map/while/body/eval_jaxpr/while/body/reduce_sum | solution.py:41
  73.8 1.6 %fusion.35 = f32[4,512,64]{1,2,0:T(8,128)S(1)} fusion(f32[4,512,512]{2,1,0:T(8,128)S(1)} %get-tuple-element.369, f32[4,512]{1,0:T(4,128)S(1)} %max.4, f32[4,512]{1,0:T(4,128)S(1)} %dynamic-slice_bitcast_fusion.8, f32[4,512]{1,0:T(4,128)S(1)} %get-tuple-element.413, pred[512,512]{0,1:T(8,128)(4,1)S(1)} %broadcast_compare_fusion.2, ...), kind=kOutput, calls=%fused_computation.8.clone.1 | convolution fusion | flops 140771328 | bytes 5799940 | tf_op jit(solution)/shard_map/while/body/eval_jaxpr/while/body/hqk,khe->hqe/dot_general | solution.py:42
  75.7 1.3 %fusion.33 = (f32[4,512]{1,0:T(4,128)S(1)}, f32[4,512,512]{2,1,0:T(8,128)S(1)}) fusion(f32[4,512]{1,0:T(4,128)S(1)} %dynamic-slice_bitcast_fusion.8, f32[4,512]{1,0:T(4,128)S(1)} %get-tuple-element.413, pred[512,512]{0,1:T(8,128)(4,1)S(1)} %broadcast_compare_fusion.2, bf16[512,4,64]{0,2,1:T(8,128)(2,1)S(1)} %get-tuple-element.412, ...), kind=kOutput, calls=%fused_computation.5.clone.1 | convolution fusion | flops 139458560 | bytes 5005316 | tf_op jit(solution)/shard_map/while/body/eval_jaxpr/while/body/qhe,khe->hqk/dot_general | solution.py:31
  77.0 1.4 %fusion.34 = f32[4,512]{1,0:T(4,128)S(1)} fusion(f32[4,512,512]{2,1,0:T(8,128)S(1)} %get-tuple-element.369, f32[4,512]{1,0:T(4,128)S(1)} %max.4, f32[4,512]{1,0:T(4,128)S(1)} %dynamic-slice_bitcast_fusion.8, f32[4,512]{1,0:T(4,128)S(1)} %get-tuple-element.413, pred[512,512]{0,1:T(8,128)(4,1)S(1)} %broadcast_compare_fusion.2), kind=kLoop, calls=%fused_computation.4.clone.1 | loop fusion | flops 6289408 | bytes 4489216 | tf_op jit(solution)/shard_map/while/body/eval_jaxpr/while/body/reduce_sum | solution.py:41
  78.4 1.6 %fusion.35 = f32[4,512,64]{1,2,0:T(8,128)S(1)} fusion(f32[4,512,512]{2,1,0:T(8,128)S(1)} %get-tuple-element.369, f32[4,512]{1,0:T(4,128)S(1)} %max.4, f32[4,512]{1,0:T(4,128)S(1)} %dynamic-slice_bitcast_fusion.8, f32[4,512]{1,0:T(4,128)S(1)} %get-tuple-element.413, pred[512,512]{0,1:T(8,128)(4,1)S(1)} %broadcast_compare_fusion.2, ...), kind=kOutput, calls=%fused_computation.8.clone.1 | convolution fusion | flops 140771328 | bytes 5799940 | tf_op jit(solution)/shard_map/while/body/eval_jaxpr/while/body/hqk,khe->hqe/dot_general | solution.py:42
  81.4 3.8 %reduce.3 = bf16[1024,256]{1,0:T(8,128)(2,1)S(1)} reduce(bf16[1024,1,256]{2,1,0:T(2,128)(2,1)S(1)} %bitcast.92, bf16[]{:T(256)} %broadcast.54), dimensions={1}, to_apply=%bitcast.58.reduce_sub_computation | reduce | bytes 1048578
  85.4 13.2 %all_to_all.60 = bf16[4,2,32768]{2,1,0:T(2,128)(2,1)S(1)} all-to-all(bf16[4,2,32768]{2,1,0:T(2,128)(2,1)S(1)} %reshape.46), channel_id=1, replica_groups=mesh['sp'=4,'dp'=8] {'sp'}, dimensions={0} | all-to-all | bytes 1048576 | tf_op jit(solution)/shard_map/all_to_all | solution.py:70
  99.4 4.5 %fusion.20 = bf16[1,256,2112]{1,2,0:T(8,128)(2,1)} fusion(bf16[1024,2112]{0,1:T(8,128)(2,1)} %all-gather.5.cloned.1.call-done, bf16[256,1024]{0,1:T(8,128)(2,1)S(1)} %bitcast.100), kind=kOutput, calls=%fused_computation.29 | convolution fusion | flops 1107836928 | bytes 5931008 | tf_op jit(solution)/shard_map/dot_general | solution.py:77
  (79 shorter events, 10.6 us)
Async XLA Ops:
  6.5 1.0 copy-start
  6.5 13.7 %copy-start.2 = (bf16[1,256,1024]{2,1,0:T(8,128)(2,1)S(1)}, bf16[1,256,1024]{2,1,0:T(8,128)(2,1)}, u32[]{:S(2)}) copy-start(bf16[1,256,1024]{2,1,0:T(8,128)(2,1)} %param.10) | copy-start | bytes 1572868
  6.5 51.7 %all-gather.3.cloned.1.call-start = ((), (), s32[]{:S(2)}) async-start(), calls=%async_computation.4 | async-start | bytes 1216512 | tf_op jit(solution)/shard_map/all_gather | solution.py:75
  15.9 13.1 %all-to-all-start = ((bf16[4,2,32768]{2,1,0:T(2,128)(2,1)}), bf16[4,2,32768]{2,1,0:T(2,128)(2,1)S(1)}, u32[]{:S(2)}, u32[]{:S(2)}) async-start(bf16[4,2,32768]{2,1,0:T(2,128)(2,1)} %reshape.40), calls=%async_computation | async-start | bytes 1048576 | tf_op jit(solution)/shard_map/all_to_all | solution.py:65
  29.0 12.3 %all-to-all-start.1 = ((bf16[4,2,32768]{2,1,0:T(2,128)(2,1)}), bf16[4,2,32768]{2,1,0:T(2,128)(2,1)S(1)}, u32[]{:S(2)}, u32[]{:S(2)}) async-start(bf16[4,2,32768]{2,1,0:T(2,128)(2,1)} %reshape.42), calls=%async_computation.1 | async-start | bytes 1048576 | tf_op jit(solution)/shard_map/all_to_all | solution.py:66
  41.3 13.0 %all-to-all-start.2 = ((bf16[4,2,32768]{2,1,0:T(2,128)(2,1)}), bf16[4,2,32768]{2,1,0:T(2,128)(2,1)}, u32[]{:S(2)}, u32[]{:S(2)}) async-start(bf16[4,2,32768]{2,1,0:T(2,128)(2,1)} %reshape.44), calls=%async_computation.2 | async-start | bytes 1048576 | tf_op jit(solution)/shard_map/all_to_all | solution.py:67
  45.4 54.0 %all-gather.5.cloned.1.call-start = ((), (), s32[]{:S(2)}) async-start(), calls=%async_computation.5 | async-start | bytes 5406720 | tf_op jit(solution)/shard_map/all_gather | solution.py:76
  48.5 9.8 %copy-start.1 = (f32[1,4,1024]{2,1,0:T(4,128)S(1)}, f32[1,4,1024]{2,1,0:T(4,128)}, u32[]{:S(2)}) copy-start(f32[1,4,1024]{2,1,0:T(4,128)} %param.12) | copy-start | bytes 49156
  48.5 9.8 %copy-start.3 = (bf16[2,512,4,64]{1,3,2,0:T(8,128)(2,1)S(1)}, bf16[2,512,4,64]{1,3,2,0:T(8,128)(2,1)}, u32[]{:S(2)}) copy-start(bf16[2,512,4,64]{1,3,2,0:T(8,128)(2,1)} %custom-call) | copy-start | bytes 1572868
  62.5 2.7 %copy-start.4 = (bf16[2,512,4,64]{1,3,2,0:T(8,128)(2,1)S(1)}, bf16[2,512,4,64]{1,3,2,0:T(8,128)(2,1)}, u32[]{:S(2)}) copy-start(bf16[2,512,4,64]{1,3,2,0:T(8,128)(2,1)} %get-tuple-element.415) | copy-start | bytes 1572868 | tf_op jit(solution)/shard_map/while/body/eval_jaxpr/while
  71.1 2.7 %copy-start.4 = (bf16[2,512,4,64]{1,3,2,0:T(8,128)(2,1)S(1)}, bf16[2,512,4,64]{1,3,2,0:T(8,128)(2,1)}, u32[]{:S(2)}) copy-start(bf16[2,512,4,64]{1,3,2,0:T(8,128)(2,1)} %get-tuple-element.415) | copy-start | bytes 1572868 | tf_op jit(solution)/shard_map/while/body/eval_jaxpr/while
  75.7 2.7 %copy-start.4 = (bf16[2,512,4,64]{1,3,2,0:T(8,128)(2,1)S(1)}, bf16[2,512,4,64]{1,3,2,0:T(8,128)(2,1)}, u32[]{:S(2)}) copy-start(bf16[2,512,4,64]{1,3,2,0:T(8,128)(2,1)} %get-tuple-element.415) | copy-start | bytes 1572868 | tf_op jit(solution)/shard_map/while/body/eval_jaxpr/while
Sparse Core Ops, SparseCore 0:
  9.5 43.1 all-gather.2
  58.4 38.7 all-gather.4
where the time goes:
time: 111 us
  local copies, waits for them, and re-layouts  21.2 us (19%)
  other arithmetic  20.1 us (18%)
  between operations  13.7 us (12%)
  blocking collectives  13.2 us (12%)
  matrix products  13 us (12%)
  starting transfers between devices  12.1 us (11%)
  waiting for transfers between devices  10.6 us (10%)
  loops' own time  6.82 us (6%)
    unnamed x27, local copies, waits for them, and re-layouts  15.2 us
    unnamed x4, other arithmetic  15.2 us
    all_to_all x1, blocking collectives, body(): lax.all_to_all(local_out[None], 'sp', split_axis=1, concat_axis=2, tiled=...  13.2 us
    another operation x1, loops' own time, attend(): outputs = lax.map(one_block, jnp.arange(block_count, dtype=jnp.int32))  6.51 us
    all_to_all x1, waiting for transfers between devices, body(): lax.all_to_all(values, 'sp', split_axis=2, concat_axis=1, tiled=True)  5.69 us
    dot_general x3, matrix products, key_step(): jnp.einsum('hqk,khe->hqe', scores.astype(jnp.bfloat16), value_part, prefe...  4.72 us
    dot_general x1, matrix products, body(): mixed = jnp.dot(attended, whole_weight, preferred_element_type=jnp.float32)  4.5 us
    all_to_all x1, starting transfers between devices, body(): lax.all_to_all(queries, 'sp', split_axis=2, concat_axis=1, tiled=True)  4.26 us
  transfers between devices with their start and end apart: 5, of which 3 were waited for; matrix products, arithmetic and copies ran while one was open for 43% of the time, Pallas kernels for 0%

commit v1 on v0

--- a/solution.py
+++ b/solution.py
@@ -2,6 +2,13 @@
 import jax.numpy as jnp
 from jax import lax
 from jax.sharding import PartitionSpec as P
+
+
+def trade_parts(x, mesh_axis, split, join):
+    peers = lax.axis_size(mesh_axis)
+    blocks = jnp.stack(jnp.split(x, peers, axis=split), axis=0)
+    blocks = lax.all_to_all(blocks, mesh_axis, split_axis=0, concat_axis=0)
+    return jnp.concatenate(blocks, axis=join)
 
 
 def attend(query_all, key_all, value_all, gate_all):
@@ -64,7 +71,7 @@
     query_heads, key_heads, value_heads = (
         lax.all_to_all(queries, "sp", split_axis=2, concat_axis=1, tiled=True),
         lax.all_to_all(keys, "sp", split_axis=2, concat_axis=1, tiled=True),
-        lax.all_to_all(values, "sp", split_axis=2, concat_axis=1, tiled=True),
+        trade_parts(values, "sp", 2, 1),
     )
     local_out = attend(query_heads[0], key_heads[0], value_heads[0], cum_gate[0])
     attended = lax.all_to_all(local_out[None], "sp", split_axis=1, concat_axis=2, tiled=True)[0]

time: 111 us -> 106 us (0.955)
  local copies, waits for them, and re-layouts: 21.2 us -> 17.8 us
  waiting for transfers between devices: 10.6 us -> 13.1 us
  blocking collectives: 13.2 us -> 11.3 us
  other arithmetic: 20.1 us -> 18.6 us
    unnamed x27 -> x21, local copies, waits for them, and re-layouts: 15.2 us -> 10.1 us
    all_to_all x1, waiting for transfers between devices: 5.69 us -> 1.14 us  [trade_parts(): blocks = lax.all_to_all(blocks, mesh_axis, split_axis=0, concat_axis=0)]
    unnamed x4 -> x3, other arithmetic: 15.2 us -> 11.4 us
    all_to_all x1, waiting for transfers between devices: 1.66 us -> 5.33 us  [body(): lax.all_to_all(keys, 'sp', split_axis=2, concat_axis=1, tiled=True)]
    all_gather x1, waiting for transfers between devices: 0.01 us -> 3.39 us  [body(): full_rows = lax.all_gather(own_rows, 'dp', axis=1, tiled=True)]
    all_to_all x1, blocking collectives: 13.2 us -> 11.3 us  [body(): lax.all_to_all(local_out[None], 'sp', split_axis=1, concat_axis=2, tiled=...]
    dynamic_update_slice x2, other arithmetic: 0.1 us -> 1.51 us  [attend(): outputs = lax.map(one_block, jnp.arange(block_count, dtype=jnp.int32))]
    another operation x6 -> x7, local copies, waits for them, and re-layouts: 0.11 us -> 1.31 us  [the longest x1 1.2 us: trade_parts(): blocks = jnp.stack(jnp.split(x, peers, axis=split), axis=0)]
  transfers between devices with their start and end apart: 5 -> 5, of which waited for: 3 -> 4; matrix products, arithmetic and copies ran while one was open for 43% -> 41% of each run, Pallas kernels for 0% -> 0%
where the time goes in v1:
time: 106 us
  other arithmetic  18.6 us (18%)
  local copies, waits for them, and re-layouts  17.8 us (17%)
  between operations  13.6 us (13%)
  waiting for transfers between devices  13.1 us (12%)
  matrix products  13 us (12%)
  starting transfers between devices  11.4 us (11%)
  blocking collectives  11.3 us (11%)
  loops' own time  6.76 us (6%)
    unnamed x3, other arithmetic  11.4 us
    all_to_all x1, blocking collectives, body(): lax.all_to_all(local_out[None], 'sp', split_axis=1, concat_axis=2, tiled=...  11.3 us
    unnamed x21, local copies, waits for them, and re-layouts  10.1 us
    another operation x1, loops' own time, attend(): outputs = lax.map(one_block, jnp.arange(block_count, dtype=jnp.int32))  6.45 us
    all_to_all x1, waiting for transfers between devices, body(): lax.all_to_all(keys, 'sp', split_axis=2, concat_axis=1, tiled=True)  5.33 us
    dot_general x3, matrix products, key_step(): jnp.einsum('hqk,khe->hqe', scores.astype(jnp.bfloat16), value_part, prefe...  4.7 us
    dot_general x1, matrix products, body(): mixed = jnp.dot(attended, whole_weight, preferred_element_type=jnp.float32)  4.5 us
    all_to_all x1, starting transfers between devices, trade_parts(): blocks = lax.all_to_all(blocks, mesh_axis, split_axis=0, concat_axis=0)  4.26 us
  transfers between devices with their start and end apart: 5, of which 4 were waited for; matrix products, arithmetic and copies ran while one was open for 41% of the time, Pallas kernels for 0%

profile of v1, /device:TPU:0, one launch (start us, length us, event | category | flops | bytes accessed | tf_op | source)
XLA Modules:
  0.0 105.7 jit_solution(14559300406368657453)
XLA Ops:
  6.5 1.0 copy-done
  8.3 1.2 %slice_bitcast_fusion.3 = (bf16[1,1,256,256]{3,2,1,0:T(8,128)(2,1)S(1)}, bf16[1,1,256,256]{3,2,1,0:T(8,128)(2,1)S(1)}, bf16[1,1,256,256]{3,2,1,0:T(8,128)(2,1)S(1)}, bf16[1,1,256,256]{3,2,1,0:T(8,128)(2,1)S(1)}) fusion(bf16[1,256,1024]{2,1,0:T(8,128)(2,1)} %param.11), kind=kLoop, calls=%fused_computation.34 | loop fusion | bytes 1048576 | tf_op jit(solution)/shard_map/stack | solution.py:9
  9.5 0.9 pad_maximum_fusion
  10.3 4.3 %all-to-all-start.2 = ((bf16[4,1,256,256]{3,2,1,0:T(8,128)(2,1)}), bf16[4,1,256,256]{3,2,1,0:T(8,128)(2,1)S(1)}, u32[]{:S(2)}, u32[]{:S(2)}) async-start(bf16[4,1,256,256]{3,2,1,0:T(8,128)(2,1)} %pad_maximum_fusion), calls=%async_computation.2 | async-start | bytes 1048576 | tf_op jit(solution)/shard_map/all_to_all | solution.py:10
  14.6 2.4 %copy.28 = bf16[1,256,1024]{1,0,2:T(2,128)(2,1)S(1)} copy(bf16[1,256,1024]{2,1,0:T(8,128)(2,1)} %param.9) | data formatting | bytes 1048576 | tf_op args[0]
  17.6 3.8 %reduce = bf16[1024,256]{1,0:T(8,128)(2,1)S(1)} reduce(bf16[1024,1,256]{2,1,0:T(2,128)(2,1)S(1)} %bitcast.93, bf16[]{:T(256)} %broadcast.54), dimensions={1}, to_apply=%bitcast.57.reduce_sub_computation | reduce | bytes 1048578
  21.4 0.9 reshape.40
  22.3 1.1 %all-to-all-done.2 = bf16[4,1,256,256]{3,2,1,0:T(8,128)(2,1)S(1)} async-done(((bf16[4,1,256,256]{3,2,1,0:T(8,128)(2,1)}), bf16[4,1,256,256]{3,2,1,0:T(8,128)(2,1)S(1)}, u32[]{:S(2)}, u32[]{:S(2)}) %all-to-all-start.2) | async-done | bytes 524320 | tf_op jit(solution)/shard_map/all_to_all | solution.py:10
  23.4 3.5 %all-to-all-start = ((bf16[4,2,32768]{2,1,0:T(2,128)(2,1)}), bf16[4,2,32768]{2,1,0:T(2,128)(2,1)S(1)}, u32[]{:S(2)}, u32[]{:S(2)}) async-start(bf16[4,2,32768]{2,1,0:T(2,128)(2,1)} %reshape.40), calls=%async_computation | async-start | bytes 1048576 | tf_op jit(solution)/shard_map/all_to_all | solution.py:72
  27.8 3.8 %reduce.1 = bf16[1024,256]{1,0:T(8,128)(2,1)S(1)} reduce(bf16[1024,1,256]{2,1,0:T(2,128)(2,1)S(1)} %bitcast.95, bf16[]{:T(256)} %broadcast.54), dimensions={1}, to_apply=%bitcast.59.reduce_sub_computation | reduce | bytes 1048578
  31.6 0.9 reshape.42
  32.5 3.2 %all-to-all-done = bf16[4,2,32768]{2,1,0:T(2,128)(2,1)S(1)} async-done(((bf16[4,2,32768]{2,1,0:T(2,128)(2,1)}), bf16[4,2,32768]{2,1,0:T(2,128)(2,1)S(1)}, u32[]{:S(2)}, u32[]{:S(2)}) %all-to-all-start) | async-done | bytes 524320 | tf_op jit(solution)/shard_map/all_to_all | solution.py:72
  35.7 3.5 %all-to-all-start.1 = ((bf16[4,2,32768]{2,1,0:T(2,128)(2,1)}), bf16[4,2,32768]{2,1,0:T(2,128)(2,1)S(1)}, u32[]{:S(2)}, u32[]{:S(2)}) async-start(bf16[4,2,32768]{2,1,0:T(2,128)(2,1)} %reshape.42), calls=%async_computation.1 | async-start | bytes 1048576 | tf_op jit(solution)/shard_map/all_to_all | solution.py:73
  39.8 1.4 %copy.35 = bf16[2,512,4,64]{1,3,2,0:T(8,128)(2,1)} copy(bf16[2,512,4,64]{3,2,1,0:T(4,128)(2,1)S(1)} %reshape.38) | data formatting | bytes 1048576
  42.6 5.3 %all-to-all-done.1 = bf16[4,2,32768]{2,1,0:T(2,128)(2,1)S(1)} async-done(((bf16[4,2,32768]{2,1,0:T(2,128)(2,1)}), bf16[4,2,32768]{2,1,0:T(2,128)(2,1)S(1)}, u32[]{:S(2)}, u32[]{:S(2)}) %all-to-all-start.1) | async-done | bytes 524320 | tf_op jit(solution)/shard_map/all_to_all | solution.py:73
  49.4 3.4 %all-gather.3.cloned.1.call-done = bf16[256,2112]{0,1:T(8,128)(2,1)} async-done(((bf16[256,264]{0,1:T(8,128)(2,1)}), bf16[256,2112]{0,1:T(8,128)(2,1)}) %all-gather.3.cloned.1.call-update) | async-done | bytes 1081360 | tf_op jit(solution)/shard_map/all_gather | solution.py:82
  52.8 23.0 %while.29 = (s32[]{:T(128)}, bf16[2,512,4,64]{1,3,2,0:T(8,128)(2,1)}, s32[2]{0:T(128)S(1)}, bf16[2,512,4,64]{1,3,2,0:T(8,128)(2,1)S(1)}, f32[2,4,512]{2,1,0:T(4,...) while((s32[]{:T(128)}, ...), condition=%wide.region_5.6_spmd.clone.clone, body=%wide.region_0.5_spmd.clone.clone.sunk | while | flops 287052800 | bytes 19649660 | solution.py:66
  56.8 4.6 %while.30 = (s32[]{:T(128)}, f32[4,512]{1,0:T(4,128)S(1)}, f32[4,512]{1,0:T(4,128)S(1)}, f32[4,512,64]{1,2,0:T(8,128)S(1)}, s32[]{:T(128)}, /*index=5*/s32[512]{...) while((s32[]{:T(128)}, f32[4,512]{1,0:T(4,128)S(1)}, ...), condition=%wide.region_4.4_spmd, body=%wide.region_1.3_spmd.sunk | while | flops 286790144 | bytes 17768688 | solution.py:62
  57.0 1.3 %fusion.33 = (f32[4,512]{1,0:T(4,128)S(1)}, f32[4,512,512]{2,1,0:T(8,128)S(1)}) fusion(f32[4,512]{1,0:T(4,128)S(1)} %dynamic-slice_bitcast_fusion.8, f32[4,512]{1,0:T(4,128)S(1)} %get-tuple-element.417, pred[512,512]{0,1:T(8,128)(4,1)S(1)} %broadcast_compare_fusion.2, bf16[512,4,64]{0,2,1:T(8,128)(2,1)S(1)} %get-tuple-element.416, ...), kind=kOutput, calls=%fused_computation.5.clone.1 | convolution fusion | flops 139458560 | bytes 5005316 | tf_op jit(solution)/shard_map/while/body/eval_jaxpr/while/body/qhe,khe->hqk/dot_general | solution.py:38
  58.3 1.4 %fusion.34 = f32[4,512]{1,0:T(4,128)S(1)} fusion(f32[4,512,512]{2,1,0:T(8,128)S(1)} %get-tuple-element.373, f32[4,512]{1,0:T(4,128)S(1)} %max.4, f32[4,512]{1,0:T(4,128)S(1)} %dynamic-slice_bitcast_fusion.8, f32[4,512]{1,0:T(4,128)S(1)} %get-tuple-element.417, pred[512,512]{0,1:T(8,128)(4,1)S(1)} %broadcast_compare_fusion.2), kind=kLoop, calls=%fused_computation.4.clone.1 | loop fusion | flops 6289408 | bytes 4489216 | tf_op jit(solution)/shard_map/while/body/eval_jaxpr/while/body/reduce_sum | solution.py:48
  59.7 1.6 %fusion.35 = f32[4,512,64]{1,2,0:T(8,128)S(1)} fusion(f32[4,512,512]{2,1,0:T(8,128)S(1)} %get-tuple-element.373, f32[4,512]{1,0:T(4,128)S(1)} %max.4, f32[4,512]{1,0:T(4,128)S(1)} %dynamic-slice_bitcast_fusion.8, f32[4,512]{1,0:T(4,128)S(1)} %get-tuple-element.417, pred[512,512]{0,1:T(8,128)(4,1)S(1)} %broadcast_compare_fusion.2, ...), kind=kOutput, calls=%fused_computation.8.clone.1 | convolution fusion | flops 140771328 | bytes 5799940 | tf_op jit(solution)/shard_map/while/body/eval_jaxpr/while/body/hqk,khe->hqe/dot_general | solution.py:49
  66.0 9.1 %while.30 = (s32[]{:T(128)}, f32[4,512]{1,0:T(4,128)S(1)}, f32[4,512]{1,0:T(4,128)S(1)}, f32[4,512,64]{1,2,0:T(8,128)S(1)}, s32[]{:T(128)}, /*index=5*/s32[512]{...) while((s32[]{:T(128)}, f32[4,512]{1,0:T(4,128)S(1)}, ...), condition=%wide.region_4.4_spmd, body=%wide.region_1.3_spmd.sunk | while | flops 286790144 | bytes 17768688 | solution.py:62
  66.3 1.3 %fusion.33 = (f32[4,512]{1,0:T(4,128)S(1)}, f32[4,512,512]{2,1,0:T(8,128)S(1)}) fusion(f32[4,512]{1,0:T(4,128)S(1)} %dynamic-slice_bitcast_fusion.8, f32[4,512]{1,0:T(4,128)S(1)} %get-tuple-element.417, pred[512,512]{0,1:T(8,128)(4,1)S(1)} %broadcast_compare_fusion.2, bf16[512,4,64]{0,2,1:T(8,128)(2,1)S(1)} %get-tuple-element.416, ...), kind=kOutput, calls=%fused_computation.5.clone.1 | convolution fusion | flops 139458560 | bytes 5005316 | tf_op jit(solution)/shard_map/while/body/eval_jaxpr/while/body/qhe,khe->hqk/dot_general | solution.py:38
  67.6 1.4 %fusion.34 = f32[4,512]{1,0:T(4,128)S(1)} fusion(f32[4,512,512]{2,1,0:T(8,128)S(1)} %get-tuple-element.373, f32[4,512]{1,0:T(4,128)S(1)} %max.4, f32[4,512]{1,0:T(4,128)S(1)} %dynamic-slice_bitcast_fusion.8, f32[4,512]{1,0:T(4,128)S(1)} %get-tuple-element.417, pred[512,512]{0,1:T(8,128)(4,1)S(1)} %broadcast_compare_fusion.2), kind=kLoop, calls=%fused_computation.4.clone.1 | loop fusion | flops 6289408 | bytes 4489216 | tf_op jit(solution)/shard_map/while/body/eval_jaxpr/while/body/reduce_sum | solution.py:48
  69.0 1.6 %fusion.35 = f32[4,512,64]{1,2,0:T(8,128)S(1)} fusion(f32[4,512,512]{2,1,0:T(8,128)S(1)} %get-tuple-element.373, f32[4,512]{1,0:T(4,128)S(1)} %max.4, f32[4,512]{1,0:T(4,128)S(1)} %dynamic-slice_bitcast_fusion.8, f32[4,512]{1,0:T(4,128)S(1)} %get-tuple-element.417, pred[512,512]{0,1:T(8,128)(4,1)S(1)} %broadcast_compare_fusion.2, ...), kind=kOutput, calls=%fused_computation.8.clone.1 | convolution fusion | flops 140771328 | bytes 5799940 | tf_op jit(solution)/shard_map/while/body/eval_jaxpr/while/body/hqk,khe->hqe/dot_general | solution.py:49
  70.8 1.3 %fusion.33 = (f32[4,512]{1,0:T(4,128)S(1)}, f32[4,512,512]{2,1,0:T(8,128)S(1)}) fusion(f32[4,512]{1,0:T(4,128)S(1)} %dynamic-slice_bitcast_fusion.8, f32[4,512]{1,0:T(4,128)S(1)} %get-tuple-element.417, pred[512,512]{0,1:T(8,128)(4,1)S(1)} %broadcast_compare_fusion.2, bf16[512,4,64]{0,2,1:T(8,128)(2,1)S(1)} %get-tuple-element.416, ...), kind=kOutput, calls=%fused_computation.5.clone.1 | convolution fusion | flops 139458560 | bytes 5005316 | tf_op jit(solution)/shard_map/while/body/eval_jaxpr/while/body/qhe,khe->hqk/dot_general | solution.py:38
  72.1 1.4 %fusion.34 = f32[4,512]{1,0:T(4,128)S(1)} fusion(f32[4,512,512]{2,1,0:T(8,128)S(1)} %get-tuple-element.373, f32[4,512]{1,0:T(4,128)S(1)} %max.4, f32[4,512]{1,0:T(4,128)S(1)} %dynamic-slice_bitcast_fusion.8, f32[4,512]{1,0:T(4,128)S(1)} %get-tuple-element.417, pred[512,512]{0,1:T(8,128)(4,1)S(1)} %broadcast_compare_fusion.2), kind=kLoop, calls=%fused_computation.4.clone.1 | loop fusion | flops 6289408 | bytes 4489216 | tf_op jit(solution)/shard_map/while/body/eval_jaxpr/while/body/reduce_sum | solution.py:48
  73.5 1.6 %fusion.35 = f32[4,512,64]{1,2,0:T(8,128)S(1)} fusion(f32[4,512,512]{2,1,0:T(8,128)S(1)} %get-tuple-element.373, f32[4,512]{1,0:T(4,128)S(1)} %max.4, f32[4,512]{1,0:T(4,128)S(1)} %dynamic-slice_bitcast_fusion.8, f32[4,512]{1,0:T(4,128)S(1)} %get-tuple-element.417, pred[512,512]{0,1:T(8,128)(4,1)S(1)} %broadcast_compare_fusion.2, ...), kind=kOutput, calls=%fused_computation.8.clone.1 | convolution fusion | flops 140771328 | bytes 5799940 | tf_op jit(solution)/shard_map/while/body/eval_jaxpr/while/body/hqk,khe->hqe/dot_general | solution.py:49
  75.9 1.6 %copy.42 = bf16[2,512,4,64]{3,2,1,0:T(4,128)(2,1)S(1)} copy(bf16[2,512,4,64]{1,3,2,0:T(8,128)(2,1)} %get-tuple-element.478) | data formatting | bytes 1048576 | tf_op jit(solution)/shard_map/broadcast_in_dim;reshape | solution.py:77
  78.2 3.8 %reduce.2 = bf16[1024,256]{1,0:T(8,128)(2,1)S(1)} reduce(bf16[1024,1,256]{2,1,0:T(2,128)(2,1)S(1)} %bitcast.94, bf16[]{:T(256)} %broadcast.54), dimensions={1}, to_apply=%bitcast.61.reduce_sub_computation | reduce | bytes 1048578
  82.1 11.3 %all_to_all.50 = bf16[4,2,32768]{2,1,0:T(2,128)(2,1)S(1)} all-to-all(bf16[4,2,32768]{2,1,0:T(2,128)(2,1)S(1)} %reshape.44), channel_id=1, replica_groups=mesh['sp'=4,'dp'=8] {'sp'}, dimensions={0} | all-to-all | bytes 1048576 | tf_op jit(solution)/shard_map/all_to_all | solution.py:77
  94.3 4.5 %fusion.20 = bf16[1,256,2112]{1,2,0:T(8,128)(2,1)} fusion(bf16[1024,2112]{0,1:T(8,128)(2,1)} %all-gather.5.cloned.1.call-done, bf16[256,1024]{0,1:T(8,128)(2,1)S(1)} %bitcast.100), kind=kOutput, calls=%fused_computation.29 | convolution fusion | flops 1107836928 | bytes 5931008 | tf_op jit(solution)/shard_map/dot_general | solution.py:84
  (73 shorter events, 10.9 us)
Async XLA Ops:
  6.5 1.0 copy-start
  6.5 46.2 %all-gather.3.cloned.1.call-start = ((), (), s32[]{:S(2)}) async-start(), calls=%async_computation.4 | async-start | bytes 1216512 | tf_op jit(solution)/shard_map/all_gather | solution.py:82
  8.3 18.6 %copy-start.2 = (bf16[1,256,1024]{2,1,0:T(8,128)(2,1)S(1)}, bf16[1,256,1024]{2,1,0:T(8,128)(2,1)}, u32[]{:S(2)}) copy-start(bf16[1,256,1024]{2,1,0:T(8,128)(2,1)} %param.10) | copy-start | bytes 1572868
  10.3 13.1 %all-to-all-start.2 = ((bf16[4,1,256,256]{3,2,1,0:T(8,128)(2,1)}), bf16[4,1,256,256]{3,2,1,0:T(8,128)(2,1)S(1)}, u32[]{:S(2)}, u32[]{:S(2)}) async-start(bf16[4,1,256,256]{3,2,1,0:T(8,128)(2,1)} %pad_maximum_fusion), calls=%async_computation.2 | async-start | bytes 1048576 | tf_op jit(solution)/shard_map/all_to_all | solution.py:10
  23.4 12.3 %all-to-all-start = ((bf16[4,2,32768]{2,1,0:T(2,128)(2,1)}), bf16[4,2,32768]{2,1,0:T(2,128)(2,1)S(1)}, u32[]{:S(2)}, u32[]{:S(2)}) async-start(bf16[4,2,32768]{2,1,0:T(2,128)(2,1)} %reshape.40), calls=%async_computation | async-start | bytes 1048576 | tf_op jit(solution)/shard_map/all_to_all | solution.py:72
  35.7 12.3 %all-to-all-start.1 = ((bf16[4,2,32768]{2,1,0:T(2,128)(2,1)}), bf16[4,2,32768]{2,1,0:T(2,128)(2,1)S(1)}, u32[]{:S(2)}, u32[]{:S(2)}) async-start(bf16[4,2,32768]{2,1,0:T(2,128)(2,1)} %reshape.42), calls=%async_computation.1 | async-start | bytes 1048576 | tf_op jit(solution)/shard_map/all_to_all | solution.py:73
  39.2 55.1 %all-gather.5.cloned.1.call-start = ((), (), s32[]{:S(2)}) async-start(), calls=%async_computation.5 | async-start | bytes 5406720 | tf_op jit(solution)/shard_map/all_gather | solution.py:83
  42.5 10.3 %copy-start.1 = (f32[1,4,1024]{2,1,0:T(4,128)S(1)}, f32[1,4,1024]{2,1,0:T(4,128)}, u32[]{:S(2)}) copy-start(f32[1,4,1024]{2,1,0:T(4,128)} %param.12) | copy-start | bytes 49156
  57.0 2.7 %copy-start.3 = (bf16[2,512,4,64]{1,3,2,0:T(8,128)(2,1)S(1)}, bf16[2,512,4,64]{1,3,2,0:T(8,128)(2,1)}, u32[]{:S(2)}) copy-start(bf16[2,512,4,64]{1,3,2,0:T(8,128)(2,1)} %get-tuple-element.419) | copy-start | bytes 1572868 | tf_op jit(solution)/shard_map/while/body/eval_jaxpr/while
  66.3 2.7 %copy-start.3 = (bf16[2,512,4,64]{1,3,2,0:T(8,128)(2,1)S(1)}, bf16[2,512,4,64]{1,3,2,0:T(8,128)(2,1)}, u32[]{:S(2)}) copy-start(bf16[2,512,4,64]{1,3,2,0:T(8,128)(2,1)} %get-tuple-element.419) | copy-start | bytes 1572868 | tf_op jit(solution)/shard_map/while/body/eval_jaxpr/while
  70.8 2.7 %copy-start.3 = (bf16[2,512,4,64]{1,3,2,0:T(8,128)(2,1)S(1)}, bf16[2,512,4,64]{1,3,2,0:T(8,128)(2,1)}, u32[]{:S(2)}) copy-start(bf16[2,512,4,64]{1,3,2,0:T(8,128)(2,1)} %get-tuple-element.419) | copy-start | bytes 1572868 | tf_op jit(solution)/shard_map/while/body/eval_jaxpr/while
Sparse Core Ops, SparseCore 0:
  9.5 43.2 all-gather.2
  54.3 34.4 all-gather.4
